TPU v7x, 32 devices: a whole 2x2x4 slice. The times are simulated.
32 devices in a mesh: tp: 4 (over y, x), dp: 8 (over z, core).
Axes of the slice: x: 2, y: 2, z: 4, core: 2. Of those that a mesh axis runs over, the one named last changes fastest.
Arguments:
- tokens: bfloat16 [64, 4096], P('tp', 'dp'), may hold values from -12 to 12, as said below
- norm_gain: float32 [2, 4096], P(None, 'dp'), may hold values from 0.1 to 1.9
- w_input: bfloat16 [2, 4096, 2048], P(None, 'dp', 'tp'), may hold values from -0.09375 to 0.09375
- w_gate: bfloat16 [2, 4096, 2048], P(None, 'dp', 'tp'), may hold values from -0.09375 to 0.09375
- w_recur: bfloat16 [2, 16, 128, 128], P(None, 'tp'), may hold values from -0.5 to 0.5
- w_inject: bfloat16 [2, 16, 128, 128], P(None, 'tp'), may hold values from -0.5 to 0.5
- conv_weight: bfloat16 [2, 4, 2048], P(None, None, 'tp'), may hold values from -3 to 3
- decay_param: float32 [2, 2048], P(None, 'tp'), may hold values from -2 to 5
- w_output: bfloat16 [2, 2048, 4096], P(None, 'tp', 'dp'), may hold values from -0.125 to 0.125
- lengths: int32 [64], P('dp'), may hold values from 1 to 48, 512 in all
- conv_state: bfloat16 [2, 3, 64, 2048], P(None, None, 'dp', 'tp'), may hold values from -6 to 6
- rec_state: float32 [2, 64, 2048], P(None, 'dp', 'tp'), may hold values from -6 to 6
Outputs:
- mixed: bfloat16 [64, 4096], P('tp', 'dp')
- new_conv: bfloat16 [2, 3, 64, 2048], P(None, None, 'dp', 'tp')
- new_rec: float32 [2, 64, 2048], P(None, 'dp', 'tp')
Inputs may be any that keep to these rules, and one draw needn't show every extreme that they name: `tokens`: activations; feature scales vary.
All inputs are finite; a program needn't handle non-finite values. No bound on the sum of `lengths` on one device may be relied on, other than what follows from the above.
Results may differ from a plain program's by a relative error of at most 0.02.
Values may be sent and summed in bfloat16 or wider, within the bound.
A program may use at most 64 MiB of HBM per device.

v0:
```python
import jax
import jax.numpy as jnp
from jax import lax
from jax.sharding import PartitionSpec as P

D = 4096


EPS = 1e-06


def body(
    tokens,
    norm_gain,
    w_input,
    w_gate,
    w_recur,
    w_inject,
    conv_weight,
    decay_param,
    w_output,
    lengths,
    conv_state,
    rec_state,
):
    state_rows = lengths.shape[0]
    live_len = lengths[:, None]
    offset = lax.axis_index("dp") * state_rows
    current = tokens
    conv_list = []
    rec_list = []
    for layer_idx in range(w_input.shape[0]):
        widened = current.astype(jnp.float32)
        squares = jnp.sum(widened * widened, axis=1)
        summed = lax.psum(squares, "dp")
        scale_rows = lax.rsqrt(summed / D + EPS)
        gathered, scale_all = (
            lax.all_gather(current, "tp", axis=0, tiled=True),
            lax.all_gather(scale_rows.astype(jnp.bfloat16), "tp", axis=0, tiled=True).astype(
                scale_rows.dtype
            ),
        )
        scaled = (gathered.astype(jnp.float32) * norm_gain[layer_idx]).astype(jnp.bfloat16)
        part_value = jnp.dot(scaled, w_input[layer_idx], preferred_element_type=jnp.float32)
        part_gate = jnp.dot(scaled, w_gate[layer_idx], preferred_element_type=jnp.float32)
        sum_value, sum_gate = (
            lax.psum_scatter(
                part_value.astype(jnp.bfloat16), "dp", scatter_dimension=0, tiled=True
            ).astype(jnp.float32),
            lax.psum_scatter(
                part_gate.astype(jnp.bfloat16), "dp", scatter_dimension=0, tiled=True
            ).astype(jnp.float32),
        )
        own_scale = lax.dynamic_slice_in_dim(scale_all, offset, state_rows, 0)
        value_in = sum_value * own_scale[:, None]
        gate_in = sum_gate * own_scale[:, None]
        conv_taps = conv_weight[layer_idx].astype(jnp.float32)
        old_taps = conv_state[layer_idx]
        tap_count = old_taps.shape[0]
        conv_out = conv_taps[tap_count] * value_in
        for back in range(1, tap_count + 1):
            conv_out = conv_out + conv_taps[tap_count - back] * jnp.where(
                back < live_len, old_taps[tap_count - back].astype(jnp.float32), jnp.float32(0.0)
            )
        local_blocks = w_recur.shape[1]
        block_width = w_recur.shape[2]
        conv_low = conv_out.astype(jnp.bfloat16).reshape(state_rows, local_blocks, block_width)
        rec_gate = jax.nn.sigmoid(
            jnp.einsum(
                "bnc,ncd->bnd", conv_low, w_recur[layer_idx], preferred_element_type=jnp.float32
            ).reshape(state_rows, -1)
        )
        inp_gate = jax.nn.sigmoid(
            jnp.einsum(
                "bnc,ncd->bnd", conv_low, w_inject[layer_idx], preferred_element_type=jnp.float32
            ).reshape(state_rows, -1)
        )
        log_decay = -8.0 * rec_gate * jax.nn.softplus(-decay_param[layer_idx])
        previous = jnp.where(live_len > 1, rec_state[layer_idx], jnp.float32(0.0))
        hidden = jnp.exp(log_decay) * previous + jnp.sqrt(-jnp.expm1(2.0 * log_decay)) * (
            inp_gate * conv_out
        )
        readout = (hidden * jax.nn.gelu(gate_in)).astype(jnp.bfloat16)
        readouts = lax.all_gather(readout, "dp", axis=0, tiled=True)
        out_weight = w_output[layer_idx]
        own_rows = lax.all_to_all(readouts, "tp", split_axis=0, concat_axis=1, tiled=True)
        branch = jnp.dot(
            own_rows,
            lax.all_gather(out_weight, "tp", axis=0, tiled=True),
            preferred_element_type=jnp.float32,
        )
        current = (widened + branch).astype(jnp.bfloat16)
        conv_list.append(
            jnp.concatenate([old_taps[1:], value_in.astype(jnp.bfloat16)[None]], axis=0)
        )
        rec_list.append(hidden)
    return (current, jnp.stack(conv_list), jnp.stack(rec_list))


def solution(mesh):
    placed = (
        P("tp", "dp"),
        P(None, "dp"),
        P(None, "dp", "tp"),
        P(None, "dp", "tp"),
        P(None, "tp", None, None),
        P(None, "tp", None, None),
        P(None, None, "tp"),
        P(None, "tp"),
        P(None, "tp", "dp"),
        P("dp"),
        P(None, None, "dp", "tp"),
        P(None, "dp", "tp"),
    )
    return jax.shard_map(
        body,
        mesh=mesh,
        in_specs=placed,
        out_specs=(P("tp", "dp"), P(None, None, "dp", "tp"), P(None, "dp", "tp")),
        check_vma=False,
    )
```

profile of v0, /device:TPU:0, one launch (start us, length us, event | category | flops | bytes accessed | tf_op | source)
XLA Modules:
  0.0 208.9 jit_solution(2642015436947091104)
XLA Ops:
  8.8 9.9 %all_gather.24 = bf16[64,512]{1,0:T(8,128)(2,1)S(1)} all-gather(bf16[16,512]{1,0:T(8,128)(2,1)} %param.12), channel_id=1, replica_groups=mesh['tp'=4,'dp'=8] {'tp'}, dimensions={0}, use_global_device_ids=true | all-gather | bytes 81920 | tf_op jit(solution)/shard_map/all_gather | solution.py:38
  18.8 1.9 convolution_convert_fusion.3
  20.8 1.9 convolution_convert_fusion.2
  22.8 1.0 fusion.108
  25.3 14.9 %psum.14 = f32[16]{0:T(128)S(1)} all-reduce(f32[16]{0:T(128)S(1)} %fusion.56), channel_id=1, replica_groups=mesh['tp'=4,'dp'=8] {'dp'}, use_global_device_ids=true, to_apply=%region_2.0 | all-reduce | flops 16 | bytes 128 | tf_op jit(solution)/shard_map/psum | solution.py:35
  40.4 9.0 %all-reduce = bf16[64]{0:T(256)(128)(2,1)S(1)} all-reduce(bf16[64]{0:T(256)(128)(2,1)S(1)} %dynamic-update-slice), channel_id=1, replica_groups=mesh['tp'=4,'dp'=8] {'tp'}, use_global_device_ids=true, to_apply=%add | all-reduce | flops 64 | bytes 256
  49.6 2.1 %reduce-scatter.5.cloned.1.call-done = bf16[8,512]{1,0:T(8,128)(2,1)} async-done(((bf16[64,512]{1,0:T(8,128)(2,1)}), bf16[8,512]{1,0:T(8,128)(2,1)}) %reduce-scatter.5.cloned.1.call-update) | async-done | bytes 8208 | tf_op jit(solution)/shard_map/reduce_scatter | solution.py:47
  51.7 1.0 fusion.32
  52.7 1.0 fusion.35
  53.7 28.9 %reduce-scatter.7.cloned.1.call-done = bf16[8,512]{1,0:T(8,128)(2,1)} async-done(((bf16[64,512]{1,0:T(8,128)(2,1)}), bf16[8,512]{1,0:T(8,128)(2,1)}) %reduce-scatter.7.cloned.1.call-update) | async-done | bytes 8208 | tf_op jit(solution)/shard_map/reduce_scatter | solution.py:50
  83.4 14.0 %all_gather.26 = bf16[64,512]{1,0:T(8,128)(2,1)S(1)} all-gather(bf16[8,512]{1,0:T(8,128)(2,1)S(1)} %get-tuple-element.22), channel_id=1, replica_groups=mesh['tp'=4,'dp'=8] {'dp'}, dimensions={0}, use_global_device_ids=true | all-gather | bytes 73728 | tf_op jit(solution)/shard_map/all_gather | solution.py:84
  97.4 8.4 %all_to_all.38 = bf16[4,16,512]{2,1,0:T(8,128)(2,1)S(1)} all-to-all(bf16[4,16,512]{2,1,0:T(8,128)(2,1)S(1)} %bitcast.206), channel_id=1, replica_groups=mesh['tp'=4,'dp'=8] {'tp'}, dimensions={0} | all-to-all | bytes 131072 | tf_op jit(solution)/shard_map/all_to_all | solution.py:86
  105.8 2.1 fusion.57
  107.8 7.5 %all_gather.28 = bf16[64,512]{1,0:T(8,128)(2,1)S(1)} all-gather(bf16[16,512]{1,0:T(8,128)(2,1)S(1)} %get-tuple-element.29), channel_id=1, replica_groups=mesh['tp'=4,'dp'=8] {'tp'}, dimensions={0}, use_global_device_ids=true | all-gather | bytes 81920 | tf_op jit(solution)/shard_map/all_gather | solution.py:38
  117.8 13.6 %psum.15 = f32[16]{0:T(128)S(1)} all-reduce(f32[16]{0:T(128)S(1)} %get-tuple-element.28), channel_id=1, replica_groups=mesh['tp'=4,'dp'=8] {'dp'}, use_global_device_ids=true, to_apply=%region_6.7 | all-reduce | flops 16 | bytes 128 | tf_op jit(solution)/shard_map/psum | solution.py:35
  131.6 9.0 %all-reduce.1 = bf16[64]{0:T(256)(128)(2,1)S(1)} all-reduce(bf16[64]{0:T(256)(128)(2,1)S(1)} %dynamic-update-slice.1), channel_id=1, replica_groups=mesh['tp'=4,'dp'=8] {'tp'}, use_global_device_ids=true, to_apply=%add.1 | all-reduce | flops 64 | bytes 256
  140.7 3.4 %reduce-scatter.9.cloned.1.call-done = bf16[8,512]{1,0:T(8,128)(2,1)} async-done(((bf16[64,512]{1,0:T(8,128)(2,1)}), bf16[8,512]{1,0:T(8,128)(2,1)}) %reduce-scatter.9.cloned.1.call-update) | async-done | bytes 8208 | tf_op jit(solution)/shard_map/reduce_scatter | solution.py:47
  144.1 0.9 fusion.36
  145.0 1.0 fusion.39
  146.0 28.9 %reduce-scatter.11.cloned.1.call-done = bf16[8,512]{1,0:T(8,128)(2,1)} async-done(((bf16[64,512]{1,0:T(8,128)(2,1)}), bf16[8,512]{1,0:T(8,128)(2,1)}) %reduce-scatter.11.cloned.1.call-update) | async-done | bytes 8208 | tf_op jit(solution)/shard_map/reduce_scatter | solution.py:50
  175.7 15.0 %all_gather.30 = bf16[64,512]{1,0:T(8,128)(2,1)} all-gather(bf16[8,512]{1,0:T(8,128)(2,1)S(1)} %get-tuple-element.24), channel_id=1, replica_groups=mesh['tp'=4,'dp'=8] {'dp'}, dimensions={0}, use_global_device_ids=true | all-gather | bytes 73728 | tf_op jit(solution)/shard_map/all_gather | solution.py:84
  190.7 3.7 %all-to-all-start.1 = ((bf16[4,16,512]{2,1,0:T(8,128)(2,1)}), bf16[4,16,512]{2,1,0:T(8,128)(2,1)S(1)}, u32[]{:S(2)}, u32[]{:S(2)}) async-start(bf16[4,16,512]{2,1,0:T(8,128)(2,1)} %bitcast.42), calls=%async_computation.5 | async-start | bytes 131072 | tf_op jit(solution)/shard_map/all_to_all | solution.py:86
  195.6 3.6 %all-to-all-done.1 = bf16[4,16,512]{2,1,0:T(8,128)(2,1)S(1)} async-done(((bf16[4,16,512]{2,1,0:T(8,128)(2,1)}), bf16[4,16,512]{2,1,0:T(8,128)(2,1)S(1)}, u32[]{:S(2)}, u32[]{:S(2)}) %all-to-all-start.1) | async-done | bytes 65568 | tf_op jit(solution)/shard_map/all_to_all | solution.py:86
  199.2 2.6 %fusion.10 = bf16[16,512]{1,0:T(8,128)(2,1)} fusion(bf16[16,2048]{1,0:T(8,128)(2,1)S(1)} %bitcast.204, bf16[1,2048,512]{2,1,0:T(8,128)(2,1)} %all-gather.7.cloned.1.call-done, bf16[16,512]{1,0:T(8,128)(2,1)S(1)} %get-tuple-element.29), kind=kOutput, calls=%fused_computation.10 | convolution fusion | flops 33579008 | bytes 2195456 | tf_op jit(solution)/shard_map/dot_general | solution.py:87
  (64 shorter events, 7.7 us)
Async XLA Ops:
  8.0 14.8 %copy-start = (bf16[2,512,512]{2,1,0:T(8,128)(2,1)S(1)}, bf16[2,512,512]{2,1,0:T(8,128)(2,1)}, u32[]{:S(2)}) copy-start(bf16[2,512,512]{2,1,0:T(8,128)(2,1)} %param.20) | copy-start | bytes 3145732
  8.0 43.7 %reduce-scatter.5.cloned.1.call-start = ((), (), s32[]{:S(2)}) async-start(), calls=%async_computation.6 | async-start | bytes 73728 | tf_op jit(solution)/shard_map/reduce_scatter | solution.py:47
  18.7 5.2 %copy-start.11 = (u32[32]{0:T(128)S(1)}, u32[32]{0:T(128)}, u32[]{:S(2)}) copy-start(u32[32]{0:T(128)} %constant.41) | copy-start | bytes 388
  18.7 6.4 %copy-start.1 = (bf16[16,512]{1,0:T(8,128)(2,1)S(1)}, bf16[16,512]{1,0:T(8,128)(2,1)}, u32[]{:S(2)}) copy-start(bf16[16,512]{1,0:T(8,128)(2,1)} %param.12) | copy-start | bytes 49156
  18.7 30.8 %copy-start.5 = (s32[8]{0:T(128)S(1)}, s32[8]{0:T(128)}, u32[]{:S(2)}) copy-start(s32[8]{0:T(128)} %param.21) | copy-start | bytes 100
  18.7 30.8 %copy-start.4 = (f32[2,512]{1,0:T(2,128)S(1)}, f32[2,512]{1,0:T(2,128)}, u32[]{:S(2)}) copy-start(f32[2,512]{1,0:T(2,128)} %param.19) | copy-start | bytes 12292
  18.7 30.8 %copy-start.3 = (bf16[2,4,512]{2,1,0:T(4,128)(2,1)S(1)}, bf16[2,4,512]{2,1,0:T(4,128)(2,1)}, u32[]{:S(2)}) copy-start(bf16[2,4,512]{2,1,0:T(4,128)(2,1)} %param.18) | copy-start | bytes 24580
  18.8 32.9 %copy-start.2 = (bf16[2,3,8,512]{3,2,1,0:T(8,128)(2,1)S(1)}, bf16[2,3,8,512]{3,2,1,0:T(8,128)(2,1)}, u32[]{:S(2)}) copy-start(bf16[2,3,8,512]{3,2,1,0:T(8,128)(2,1)} %param.22) | copy-start | bytes 147460
  18.8 32.9 %copy-start.8 = (bf16[2,4,128,128]{3,2,1,0:T(8,128)(2,1)S(1)}, bf16[2,4,128,128]{3,2,1,0:T(8,128)(2,1)}, u32[]{:S(2)}) copy-start(bf16[2,4,128,128]{3,2,1,0:T(8,128)(2,1)} %param.16) | copy-start | bytes 786436
  20.7 32.0 %copy-start.9 = (bf16[2,4,128,128]{3,2,1,0:T(8,128)(2,1)S(1)}, bf16[2,4,128,128]{3,2,1,0:T(8,128)(2,1)}, u32[]{:S(2)}) copy-start(bf16[2,4,128,128]{3,2,1,0:T(8,128)(2,1)} %param.17) | copy-start | bytes 786436
  20.7 32.0 %copy-start.10 = (f32[2,8,512]{2,1,0:T(8,128)S(1)}, f32[2,8,512]{2,1,0:T(8,128)}, u32[]{:S(2)}) copy-start(f32[2,8,512]{2,1,0:T(8,128)} %param.23) | copy-start | bytes 98308
  20.7 61.8 %reduce-scatter.7.cloned.1.call-start = ((), (), s32[]{:S(2)}) async-start(), calls=%async_computation.7 | async-start | bytes 73728 | tf_op jit(solution)/shard_map/reduce_scatter | solution.py:50
  22.7 83.1 %all-gather.5.cloned.1.call-start = ((), (), s32[]{:S(2)}) async-start(), calls=%async_computation.10 | async-start | bytes 2621440 | tf_op jit(solution)/shard_map/all_gather | solution.py:89
  23.8 91.6 %copy-start.6 = (bf16[2,512,512]{2,1,0:T(8,128)(2,1)S(1)}, bf16[2,512,512]{2,1,0:T(8,128)(2,1)}, u32[]{:S(2)}) copy-start(bf16[2,512,512]{2,1,0:T(8,128)(2,1)} %param.14) | copy-start | bytes 3145732
  23.8 120.3 %reduce-scatter.9.cloned.1.call-start = ((), (), s32[]{:S(2)}) async-start(), calls=%async_computation.8 | async-start | bytes 73728 | tf_op jit(solution)/shard_map/reduce_scatter | solution.py:47
  51.7 64.6 %copy-start.7 = (bf16[2,512,512]{2,1,0:T(8,128)(2,1)S(1)}, bf16[2,512,512]{2,1,0:T(8,128)(2,1)}, u32[]{:S(2)}) copy-start(bf16[2,512,512]{2,1,0:T(8,128)(2,1)} %param.15) | copy-start | bytes 3145732
  116.2 58.7 %reduce-scatter.11.cloned.1.call-start = ((), (), s32[]{:S(2)}) async-start(), calls=%async_computation.9 | async-start | bytes 73728 | tf_op jit(solution)/shard_map/reduce_scatter | solution.py:50
  117.1 82.0 %all-gather.7.cloned.1.call-start = ((), (), s32[]{:S(2)}) async-start(), calls=%async_computation.11 | async-start | bytes 2621440 | tf_op jit(solution)/shard_map/all_gather | solution.py:89
  190.7 8.5 %all-to-all-start.1 = ((bf16[4,16,512]{2,1,0:T(8,128)(2,1)}), bf16[4,16,512]{2,1,0:T(8,128)(2,1)S(1)}, u32[]{:S(2)}, u32[]{:S(2)}) async-start(bf16[4,16,512]{2,1,0:T(8,128)(2,1)} %bitcast.42), calls=%async_computation.5 | async-start | bytes 131072 | tf_op jit(solution)/shard_map/all_to_all | solution.py:86
Sparse Core Ops, SparseCore 0:
  20.9 30.7 reduce-scatter.4
  53.9 28.6 reduce-scatter.6
  116.3 27.7 reduce-scatter.8
  146.2 28.6 reduce-scatter.10
Sparse Core Ops, SparseCore 1:
  25.0 35.3 all-gather.4
  119.5 32.3 all-gather.6
where the time goes:
time: 210 us; the launch traced here: 209 us
  blocking collectives  101 us (48%)
  waiting for transfers between devices  67.5 us (32%)
  between operations  16.1 us (8%)
  matrix products  14 us (7%)
  starting transfers between devices  3.9 us (2%)
  local copies, waits for them, and re-layouts  3.14 us (1%)
  other arithmetic  3.02 us (1%)
    reduce_scatter x2, waiting for transfers between devices, body(): lax.psum_scatter(part_gate.astype(jnp.bfloat16), 'dp', scatter_dimension=...  57.7 us
    all_gather x2, blocking collectives, body(): readouts = lax.all_gather(readout, 'dp', axis=0, tiled=True)  29 us
    psum x2, blocking collectives, body(): summed = lax.psum(squares, 'dp')  28.5 us
    unnamed x2, blocking collectives  18 us
    all_gather x2, blocking collectives, body(): lax.all_gather(current, 'tp', axis=0, tiled=True)  17.4 us
    all_to_all x1, blocking collectives, body(): lax.all_to_all(readouts, 'tp', split_axis=0, concat_axis=1, tiled=True)  8.38 us
    reduce_scatter x2, waiting for transfers between devices, body(): lax.psum_scatter(part_value.astype(jnp.bfloat16), 'dp', scatter_dimension...  5.53 us
    dot_general x2, matrix products, body(): jnp.dot(own_rows, lax.all_gather(out_weight, 'tp', axis=0, tiled=True), p...  4.67 us
  transfers between devices with their start and end apart: 7, of which 5 were waited for; matrix products, arithmetic and copies ran while one was open for 6% of the time, Pallas kernels for 0%

commit v1 on v0

v1 whole, which is shorter than its diff:
```python
import functools

import jax
import jax.numpy as jnp
from jax import lax
from jax.experimental import pallas as pl
from jax.experimental.pallas import tpu as pltpu
from jax.sharding import PartitionSpec as P

EPS = 1e-06
MESH = pl.DeviceIdType.MESH
LANES = 128


def shift_order(count):
    return sorted(range(1, count), key=lambda s: (-min(s, count - s), s))


def kernel(
    n_tp,
    n_dp,
    tokens,
    norm_gain,
    w_input,
    w_gate,
    w_recur,
    w_inject,
    conv_weight,
    decay_param,
    w_output,
    lengths,
    conv_state,
    rec_state,
    mixed,
    new_conv,
    new_rec,
    gain_v,
    win_v,
    wgate_v,
    wrec_v,
    winj_v,
    cw_v,
    decay_v,
    wout_v,
    len_s,
    cs_v,
    rs_v,
    x_all,
    x_keep,
    sq_out,
    sq_in,
    val_out,
    val_in,
    gate_out,
    gate_in_buf,
    read_all,
    part_all,
    last_out,
    last_in,
    load_sem,
    tok_send,
    tok_recv,
    sq_send,
    sq_recv,
    val_send,
    val_recv,
    gate_send,
    gate_recv,
    read_send,
    read_recv,
    part_send,
    part_recv,
):
    me_tp = lax.axis_index("tp")
    me_dp = lax.axis_index("dp")
    layers = w_input.shape[0]
    rows, width = tokens.shape
    state_rows = lengths.shape[0]
    chans = w_input.shape[2]
    taps = conv_state.shape[1]
    blocks, blk = w_recur.shape[1], w_recur.shape[2]
    all_rows = rows * n_tp
    model = width * n_dp

    loads = {}

    def load(name, src, dst, idx):
        copy = pltpu.make_async_copy(src, dst, load_sem.at[idx])
        copy.start()
        loads[name] = copy

    load("tokens", tokens, x_all.at[me_tp], 0)
    load("gain", norm_gain, gain_v, 1)
    load("win", w_input, win_v, 2)
    load("wgate", w_gate, wgate_v, 3)
    load("cw", conv_weight, cw_v, 4)
    load("decay", decay_param, decay_v, 5)
    load("len", lengths, len_s, 6)
    load("cs", conv_state, cs_v, 7)
    load("rs", rec_state, rs_v, 8)
    load("wrec", w_recur, wrec_v, 9)
    load("winj", w_inject, winj_v, 10)
    load("wout", w_output, wout_v, 11)

    barrier = pltpu.get_barrier_semaphore()
    for s in range(1, n_tp):
        pl.semaphore_signal(
            barrier, inc=1, device_id={"tp": lax.rem(me_tp + s, n_tp)}, device_id_type=MESH
        )
    for s in range(1, n_dp):
        pl.semaphore_signal(
            barrier, inc=1, device_id={"dp": lax.rem(me_dp + s, n_dp)}, device_id_type=MESH
        )
    loads["tokens"].wait()
    pl.semaphore_wait(barrier, n_tp + n_dp - 2)

    sent = []

    def send(src, dst, send_sem, recv_sem, axis, target):
        copy = pltpu.make_async_remote_copy(
            src_ref=src,
            dst_ref=dst,
            send_sem=send_sem,
            recv_sem=recv_sem,
            device_id={axis: target},
            device_id_type=MESH,
        )
        copy.start()
        sent.append(copy)
        return copy

    def gather(buf, send_sems, recv_sems, axis, me, count):
        copies = []
        for s in shift_order(count):
            copies.append(
                send(
                    buf.at[me],
                    buf.at[me],
                    send_sems.at[s],
                    recv_sems.at[s],
                    axis,
                    lax.rem(me + s, count),
                )
            )
        return copies

    def scatter(out, into, send_sems, recv_sems, axis, me, count):
        copies = []
        for s in shift_order(count):
            target = lax.rem(me + s, count)
            copies.append(
                send(out.at[target], into.at[s], send_sems.at[s], recv_sems.at[s], axis, target)
            )
        return copies

    def arrive(copies):
        for copy in copies:
            copy.wait_recv()

    tok = gather(x_all, tok_send, tok_recv, "tp", me_tp, n_tp)

    loads["len"].wait()
    row_id = lax.broadcasted_iota(jnp.int32, (state_rows, chans), 0)
    live_len = jnp.zeros((state_rows, chans), jnp.int32)
    for r in range(state_rows):
        live_len = jnp.where(row_id == r, len_s[r], live_len)
    loads["decay"].wait()
    neg = -decay_v[...]
    rate = -8.0 * (jnp.maximum(neg, 0.0) + jnp.log1p(jnp.exp(-jnp.abs(neg))))
    loads["gain"].wait()
    gains = gain_v[...]

    arrive(tok)
    current = x_all[...].astype(jnp.float32).reshape(all_rows, width)

    for l in range(layers):
        squares = None
        for c in range(0, width, LANES):
            piece = current[:, c : c + LANES]
            squares = piece * piece if squares is None else squares + piece * piece
        sq_out[l] = squares.reshape(n_dp, state_rows, LANES)
        sq_copies = scatter(
            sq_out.at[l], sq_in.at[l], sq_send.at[l], sq_recv.at[l], "dp", me_dp, n_dp
        )
        scaled = (current * gains[l : l + 1]).astype(jnp.bfloat16)
        if l == 0:
            loads["win"].wait()
        part = jnp.dot(scaled, win_v[l], preferred_element_type=jnp.float32)
        val_out[l] = part.reshape(n_dp, state_rows, chans).astype(jnp.bfloat16)
        val_copies = scatter(
            val_out.at[l], val_in.at[l], val_send.at[l], val_recv.at[l], "dp", me_dp, n_dp
        )
        if l == 0:
            loads["wgate"].wait()
        part = jnp.dot(scaled, wgate_v[l], preferred_element_type=jnp.float32)
        gate_out[l] = part.reshape(n_dp, state_rows, chans).astype(jnp.bfloat16)
        gate_copies = scatter(
            gate_out.at[l], gate_in_buf.at[l], gate_send.at[l], gate_recv.at[l], "dp", me_dp, n_dp
        )

        if l == 0:
            for name in ("cw", "cs", "rs", "wrec", "winj"):
                loads[name].wait()
        conv_taps = cw_v[l].astype(jnp.float32)
        old = [cs_v[l, t].astype(jnp.float32) for t in range(taps)]
        history = jnp.zeros((state_rows, chans), jnp.float32)
        for back in range(1, taps + 1):
            history = history + conv_taps[taps - back : taps - back + 1] * jnp.where(
                back < live_len, old[taps - back], 0.0
            )
        previous = jnp.where(live_len > 1, rs_v[l], 0.0)
        for t in range(1, taps):
            new_conv[l, t - 1] = cs_v[l, t]

        arrive(sq_copies)
        total = sq_out[l, me_dp]
        for s in range(1, n_dp):
            total = total + sq_in[l, s]
        scale = lax.rsqrt(jnp.sum(total, axis=1, keepdims=True) / model + EPS)
        arrive(val_copies)
        value = val_out[l, me_dp].astype(jnp.float32)
        for s in range(1, n_dp):
            value = value + val_in[l, s].astype(jnp.float32)
        value = value * scale
        new_conv[l, taps - 1] = value.astype(jnp.bfloat16)
        conv_out = conv_taps[taps : taps + 1] * value + history
        conv_low = conv_out.astype(jnp.bfloat16)
        rec_parts = []
        inj_parts = []
        for b in range(blocks):
            piece = conv_low[:, b * blk : (b + 1) * blk]
            rec_parts.append(jnp.dot(piece, wrec_v[l, b], preferred_element_type=jnp.float32))
            inj_parts.append(jnp.dot(piece, winj_v[l, b], preferred_element_type=jnp.float32))
        rec_gate = jax.nn.sigmoid(jnp.concatenate(rec_parts, axis=1))
        inp_gate = jax.nn.sigmoid(jnp.concatenate(inj_parts, axis=1))
        log_decay = rate[l : l + 1] * rec_gate
        half = jnp.tanh(log_decay)
        hidden = jnp.exp(log_decay) * previous + jnp.sqrt(-2.0 * half / (1.0 - half)) * (
            inp_gate * conv_out
        )
        new_rec[l] = hidden
        arrive(gate_copies)
        gate = gate_out[l, me_dp].astype(jnp.float32)
        for s in range(1, n_dp):
            gate = gate + gate_in_buf[l, s].astype(jnp.float32)
        gate = gate * scale
        read_all[l, me_dp] = (hidden * jax.nn.gelu(gate)).astype(jnp.bfloat16)
        arrive(
            gather(read_all.at[l], read_send.at[l], read_recv.at[l], "dp", me_dp, n_dp)
        )
        reads = read_all[l].astype(jnp.float32).reshape(all_rows, chans).astype(jnp.bfloat16)
        if l == 0:
            loads["wout"].wait()
        branch = jnp.dot(reads, wout_v[l], preferred_element_type=jnp.float32)
        if l < layers - 1:
            part_all[l, me_tp] = branch.astype(jnp.bfloat16)
            arrive(
                gather(part_all.at[l], part_send.at[l], part_recv.at[l], "tp", me_tp, n_tp)
            )
            for j in range(n_tp):
                current = current + part_all[l, j].astype(jnp.float32)
            current = current.astype(jnp.bfloat16)
            x_keep[...] = current.reshape(n_tp, rows, width)
            current = current.astype(jnp.float32)
        else:
            last_out[...] = branch.reshape(n_tp, rows, width).astype(jnp.bfloat16)
            arrive(
                scatter(last_out, last_in, part_send.at[l], part_recv.at[l], "tp", me_tp, n_tp)
            )
            final = (x_keep if l else x_all)[me_tp].astype(jnp.float32) + last_out[me_tp].astype(jnp.float32)
            for s in range(1, n_tp):
                final = final + last_in[s].astype(jnp.float32)
            mixed[...] = final.astype(jnp.bfloat16)
    for copy in sent:
        copy.wait_send()


def body(n_tp, n_dp, *args):
    (tokens, norm_gain, w_input, w_gate, w_recur, w_inject, conv_weight, decay_param, w_output,
     lengths, conv_state, rec_state) = args
    layers = w_input.shape[0]
    rows, width = tokens.shape
    state_rows = lengths.shape[0]
    chans = w_input.shape[2]
    all_rows = rows * n_tp
    bf16, f32 = jnp.bfloat16, jnp.float32
    like = lambda a: pltpu.VMEM(a.shape, a.dtype)
    dma = pltpu.SemaphoreType.DMA
    vmem = pl.BlockSpec(memory_space=pltpu.VMEM)
    return pl.pallas_call(
        functools.partial(kernel, n_tp, n_dp),
        out_shape=(
            jax.ShapeDtypeStruct(tokens.shape, bf16),
            jax.ShapeDtypeStruct(conv_state.shape, bf16),
            jax.ShapeDtypeStruct(rec_state.shape, f32),
        ),
        in_specs=[pl.BlockSpec(memory_space=pl.ANY)] * len(args),
        out_specs=(vmem, vmem, vmem),
        scratch_shapes=[
            like(norm_gain),
            like(w_input),
            like(w_gate),
            like(w_recur),
            like(w_inject),
            like(conv_weight),
            like(decay_param),
            like(w_output),
            pltpu.SMEM(lengths.shape, lengths.dtype),
            like(conv_state),
            like(rec_state),
            pltpu.VMEM((n_tp, rows, width), bf16),
            pltpu.VMEM((n_tp, rows, width), bf16),
            pltpu.VMEM((layers, n_dp, state_rows, LANES), f32),
            pltpu.VMEM((layers, n_dp, state_rows, LANES), f32),
            pltpu.VMEM((layers, n_dp, state_rows, chans), bf16),
            pltpu.VMEM((layers, n_dp, state_rows, chans), bf16),
            pltpu.VMEM((layers, n_dp, state_rows, chans), bf16),
            pltpu.VMEM((layers, n_dp, state_rows, chans), bf16),
            pltpu.VMEM((layers, n_dp, state_rows, chans), bf16),
            pltpu.VMEM((layers, n_tp, all_rows, width), bf16),
            pltpu.VMEM((n_tp, rows, width), bf16),
            pltpu.VMEM((n_tp, rows, width), bf16),
            dma((12,)),
            dma((n_tp,)),
            dma((n_tp,)),
            dma((layers, n_dp)),
            dma((layers, n_dp)),
            dma((layers, n_dp)),
            dma((layers, n_dp)),
            dma((layers, n_dp)),
            dma((layers, n_dp)),
            dma((layers, n_dp)),
            dma((layers, n_dp)),
            dma((layers, n_tp)),
            dma((layers, n_tp)),
        ],
        compiler_params=pltpu.CompilerParams(collective_id=0, has_side_effects=True),
    )(*args)


def solution(mesh):
    n_tp, n_dp = mesh.shape["tp"], mesh.shape["dp"]
    placed = (
        P("tp", "dp"),
        P(None, "dp"),
        P(None, "dp", "tp"),
        P(None, "dp", "tp"),
        P(None, "tp", None, None),
        P(None, "tp", None, None),
        P(None, None, "tp"),
        P(None, "tp"),
        P(None, "tp", "dp"),
        P("dp"),
        P(None, None, "dp", "tp"),
        P(None, "dp", "tp"),
    )
    return jax.shard_map(
        functools.partial(body, n_tp, n_dp),
        mesh=mesh,
        in_specs=placed,
        out_specs=(P("tp", "dp"), P(None, None, "dp", "tp"), P(None, "dp", "tp")),
        check_vma=False,
    )
```

time: 210 us -> 41.6 us (0.20)
  blocking collectives: 101 us -> 0 us
  waiting for transfers between devices: 67.5 us -> 0 us
  Pallas kernels: 0 us -> 37.2 us
  between operations: 16.1 us -> 0.65 us
  matrix products: 14 us -> 0 us
  starting transfers between devices: 3.9 us -> 0 us
  other arithmetic: 3.02 us -> 0 us
    reduce_scatter x4 -> x0, waiting for transfers between devices: 63.2 us -> none  [the longest x2 57.7 us: body(): lax.psum_scatter(part_gate.astype(jnp.bfloat16), 'dp', scatter_dimension=...]
    all_gather x4 -> x0, blocking collectives: 46.4 us -> none  [the longest x2 29 us: body(): readouts = lax.all_gather(readout, 'dp', axis=0, tiled=True)]
    pallas_call x0 -> x1, Pallas kernels: none -> 37.2 us  [body(): pl.pallas_call(functools.partial(kernel, n_tp, n_dp), out_shape=(jax.Shap...]
    psum x2 -> x0, blocking collectives: 28.5 us -> none  [body(): summed = lax.psum(squares, 'dp')]
    unnamed x2 -> x0, blocking collectives: 18 us -> none
    dot_general x10 -> x0, matrix products: 14 us -> none  [the longest x2 4.67 us: body(): jnp.dot(own_rows, lax.all_gather(out_weight, 'tp', axis=0, tiled=True), p...]
    all_to_all x1 -> x0, blocking collectives: 8.38 us -> none  [body(): lax.all_to_all(readouts, 'tp', split_axis=0, concat_axis=1, tiled=True)]
    all_to_all x1 -> x0, starting transfers between devices: 3.65 us -> none  [body(): lax.all_to_all(readouts, 'tp', split_axis=0, concat_axis=1, tiled=True)]
  transfers between devices with their start and end apart: 7 -> 0, of which waited for: 5 -> 0; matrix products, arithmetic and copies ran while one was open for 6% -> 0% of each run, Pallas kernels for 0% -> 0%
where the time goes in v1:
time: 41.6 us; the launch traced here: 41.2 us
  Pallas kernels  37.2 us (89%)
  local copies, waits for them, and re-layouts  3.37 us (8%)
  between operations  0.65 us (2%)
    pallas_call x1, Pallas kernels, body(): pl.pallas_call(functools.partial(kernel, n_tp, n_dp), out_shape=(jax.Shap...  37.2 us
    unnamed x5, local copies, waits for them, and re-layouts  3.37 us

profile of v1, /device:TPU:0, one launch (start us, length us, event | category | flops | bytes accessed | tf_op | source)
XLA Modules:
  0.0 41.2 jit_solution(14368324467304924235)
XLA Ops:
  0.6 37.2 %shard_map.139 = (bf16[16,512]{1,0:T(8,128)(2,1)}, bf16[2,3,8,512]{3,2,1,0:T(8,128)(2,1)}, f32[2,8,512]{2,1,0:T(8,128)}) custom-call(bf16[16,512]{1,0:T(8,128)(2,1)} %tokens.1, f32[2,512]{1,0:T(2,128)} %norm_gain.1, bf16[2,512,512]{2,1,0:T(8,128)(2,1)} %w_input.1, bf16[2,512,512]{2,1,0:T(8,128)(2,1)} %w_gate.1, bf16[2,4,128,128]{3,2,1,0:T(8,128)(2,1)} %w_recur.1, ...), custom_call_target="tpu_custom_call" | custom-call | tf_op jit(solution)/shard_map/pallas_call | solution.py:290
  37.8 1.3 %copy.18 = bf16[16,512]{1,0:T(8,128)(2,1)} copy(bf16[16,512]{1,0:T(8,128)(2,1)} %get-tuple-element.6) | data formatting | bytes 32768
  39.1 0.0 copy-start
  39.1 1.4 %copy.19 = bf16[2,3,8,512]{3,2,1,0:T(8,128)(2,1)} copy(bf16[2,3,8,512]{3,2,1,0:T(8,128)(2,1)} %get-tuple-element.7) | data formatting | bytes 98304
  40.6 0.0 copy-done
  40.6 0.6 %copy.20 = f32[2,8,512]{2,1,0:T(8,128)} copy(f32[2,8,512]{2,1,0:T(8,128)S(1)} %copy-done) | data formatting | bytes 65536
Async XLA Ops:
  39.1 1.4 %copy-start = (f32[2,8,512]{2,1,0:T(8,128)S(1)}, f32[2,8,512]{2,1,0:T(8,128)}, u32[]{:S(2)}) copy-start(f32[2,8,512]{2,1,0:T(8,128)} %get-tuple-element.8) | copy-start | bytes 98308

commit v2 on v1

--- a/solution.py
+++ b/solution.py
@@ -12,8 +12,19 @@
 LANES = 128
 
 
-def shift_order(count):
-    return sorted(range(1, count), key=lambda s: (-min(s, count - s), s))
+def order_of(count):
+    return sorted(range(1, count), reverse=True)
+
+
+def partner(me, step, count):
+    if count & (count - 1):
+        return lax.rem(count + step - me, count)
+    other, bit = me, 1
+    while bit < count:
+        if step & bit:
+            other = other + bit - 2 * bit * lax.rem(me // bit, 2)
+        bit *= 2
+    return other
 
 
 def kernel(
@@ -90,6 +101,15 @@
         loads[name] = copy
 
     load("tokens", tokens, x_all.at[me_tp], 0)
+    barrier = pltpu.get_barrier_semaphore()
+    for s in range(1, n_tp):
+        pl.semaphore_signal(
+            barrier, inc=1, device_id={"tp": lax.rem(me_tp + s, n_tp)}, device_id_type=MESH
+        )
+    for s in range(1, n_dp):
+        pl.semaphore_signal(
+            barrier, inc=1, device_id={"dp": lax.rem(me_dp + s, n_dp)}, device_id_type=MESH
+        )
     load("gain", norm_gain, gain_v, 1)
     load("win", w_input, win_v, 2)
     load("wgate", w_gate, wgate_v, 3)
@@ -102,15 +122,6 @@
     load("winj", w_inject, winj_v, 10)
     load("wout", w_output, wout_v, 11)
 
-    barrier = pltpu.get_barrier_semaphore()
-    for s in range(1, n_tp):
-        pl.semaphore_signal(
-            barrier, inc=1, device_id={"tp": lax.rem(me_tp + s, n_tp)}, device_id_type=MESH
-        )
-    for s in range(1, n_dp):
-        pl.semaphore_signal(
-            barrier, inc=1, device_id={"dp": lax.rem(me_dp + s, n_dp)}, device_id_type=MESH
-        )
     loads["tokens"].wait()
     pl.semaphore_wait(barrier, n_tp + n_dp - 2)
 
@@ -131,7 +142,7 @@
 
     def gather(buf, send_sems, recv_sems, axis, me, count):
         copies = []
-        for s in shift_order(count):
+        for s in order_of(count):
             copies.append(
                 send(
                     buf.at[me],
@@ -139,15 +150,15 @@
                     send_sems.at[s],
                     recv_sems.at[s],
                     axis,
-                    lax.rem(me + s, count),
+                    partner(me, s, count),
                 )
             )
         return copies
 
     def scatter(out, into, send_sems, recv_sems, axis, me, count):
         copies = []
-        for s in shift_order(count):
-            target = lax.rem(me + s, count)
+        for s in order_of(count):
+            target = partner(me, s, count)
             copies.append(
                 send(out.at[target], into.at[s], send_sems.at[s], recv_sems.at[s], axis, target)
             )
@@ -275,6 +286,19 @@
         copy.wait_send()
 
 
+def flush(*refs):
+    count = len(refs) // 2
+    sems = refs[-1]
+    copies = [
+        pltpu.make_async_copy(src, dst, sems.at[i])
+        for i, (src, dst) in enumerate(zip(refs[:count], refs[count : 2 * count]))
+    ]
+    for copy in copies:
+        copy.start()
+    for copy in copies:
+        copy.wait()
+
+
 def body(n_tp, n_dp, *args):
     (tokens, norm_gain, w_input, w_gate, w_recur, w_inject, conv_weight, decay_param, w_output,
      lengths, conv_state, rec_state) = args
@@ -287,13 +311,10 @@
     like = lambda a: pltpu.VMEM(a.shape, a.dtype)
     dma = pltpu.SemaphoreType.DMA
     vmem = pl.BlockSpec(memory_space=pltpu.VMEM)
-    return pl.pallas_call(
+    shapes = ((tokens.shape, bf16), (conv_state.shape, bf16), (rec_state.shape, f32))
+    held = pl.pallas_call(
         functools.partial(kernel, n_tp, n_dp),
-        out_shape=(
-            jax.ShapeDtypeStruct(tokens.shape, bf16),
-            jax.ShapeDtypeStruct(conv_state.shape, bf16),
-            jax.ShapeDtypeStruct(rec_state.shape, f32),
-        ),
+        out_shape=tuple(pltpu.VMEM(*each) for each in shapes),
         in_specs=[pl.BlockSpec(memory_space=pl.ANY)] * len(args),
         out_specs=(vmem, vmem, vmem),
         scratch_shapes=[
@@ -336,6 +357,13 @@
         ],
         compiler_params=pltpu.CompilerParams(collective_id=0, has_side_effects=True),
     )(*args)
+    return pl.pallas_call(
+        flush,
+        out_shape=tuple(jax.ShapeDtypeStruct(*each) for each in shapes),
+        in_specs=[vmem] * len(shapes),
+        out_specs=tuple(pl.BlockSpec(memory_space=pl.ANY) for _ in shapes),
+        scratch_shapes=[dma((len(shapes),))],
+    )(*[pltpu.with_memory_space_constraint(each, pltpu.VMEM) for each in held])
 
 
 def solution(mesh):

time: 41.6 us -> 37.4 us (0.90)
  local copies, waits for them, and re-layouts: 3.37 us -> 0 us
  Pallas kernels: 37.2 us -> 36.5 us
    unnamed x5 -> x0, local copies, waits for them, and re-layouts: 3.37 us -> none
    pallas_call x1 -> x2, Pallas kernels: 37.2 us -> 36.5 us  [the longest x1 35.9 us: body(): pl.pallas_call(functools.partial(kernel, n_tp, n_dp), out_shape=tuple((pl...]
where the time goes in v2:
time: 37.4 us; the launch traced here: 37.2 us
  Pallas kernels  36.5 us (98%)
  between operations  0.64 us (2%)
    pallas_call x1, Pallas kernels, body(): pl.pallas_call(functools.partial(kernel, n_tp, n_dp), out_shape=tuple((pl...  35.9 us

profile of v2, /device:TPU:0, one launch (start us, length us, event | category | flops | bytes accessed | tf_op | source)
XLA Modules:
  0.0 37.2 jit_solution(12582465339590779206)
XLA Ops:
  0.6 35.9 %shard_map.139 = (bf16[16,512]{1,0:T(8,128)(2,1)S(1)}, bf16[2,3,8,512]{3,2,1,0:T(8,128)(2,1)S(1)}, f32[2,8,512]{2,1,0:T(8,128)S(1)}) custom-call(bf16[16,512]{1,0:T(8,128)(2,1)} %tokens.1, f32[2,512]{1,0:T(2,128)} %norm_gain.1, bf16[2,512,512]{2,1,0:T(8,128)(2,1)} %w_input.1, bf16[2,512,512]{2,1,0:T(8,128)(2,1)} %w_gate.1, bf16[2,4,128,128]{3,2,1,0:T(8,128)(2,1)} %w_recur.1, ...), custom_call_target="tpu_custom_call" | custom-call | tf_op jit(solution)/shard_map/pallas_call | solution.py:315
  36.5 0.7 %shard_map.140 = (bf16[16,512]{1,0:T(8,128)(2,1)}, bf16[2,3,8,512]{3,2,1,0:T(8,128)(2,1)}, f32[2,8,512]{2,1,0:T(8,128)}) custom-call(bf16[16,512]{1,0:T(8,128)(2,1)S(1)} %get-tuple-element.6.refs_0_, bf16[2,3,8,512]{3,2,1,0:T(8,128)(2,1)S(1)} %get-tuple-element.7.refs_1_, f32[2,8,512]{2,1,0:T(8,128)S(1)} %get-tuple-element.8.refs_2_), custom_call_target="tpu_custom_call" | custom-call | tf_op jit(solution)/shard_map/pallas_call | solution.py:360

commit v3 on v2

--- a/solution.py
+++ b/solution.py
@@ -81,6 +81,8 @@
     read_recv,
     part_send,
     part_recv,
+    last_send,
+    last_recv,
 ):
     me_tp = lax.axis_index("tp")
     me_dp = lax.axis_index("dp")
@@ -155,15 +157,6 @@
             )
         return copies
 
-    def scatter(out, into, send_sems, recv_sems, axis, me, count):
-        copies = []
-        for s in order_of(count):
-            target = partner(me, s, count)
-            copies.append(
-                send(out.at[target], into.at[s], send_sems.at[s], recv_sems.at[s], axis, target)
-            )
-        return copies
-
     def arrive(copies):
         for copy in copies:
             copy.wait_recv()
@@ -184,31 +177,60 @@
     arrive(tok)
     current = x_all[...].astype(jnp.float32).reshape(all_rows, width)
 
-    for l in range(layers):
+    def lane_squares(block):
         squares = None
         for c in range(0, width, LANES):
-            piece = current[:, c : c + LANES]
+            piece = block[:, c : c + LANES]
             squares = piece * piece if squares is None else squares + piece * piece
-        sq_out[l] = squares.reshape(n_dp, state_rows, LANES)
-        sq_copies = scatter(
-            sq_out.at[l], sq_in.at[l], sq_send.at[l], sq_recv.at[l], "dp", me_dp, n_dp
-        )
-        scaled = (current * gains[l : l + 1]).astype(jnp.bfloat16)
+        return squares
+
+    def dot(a, b):
+        return jnp.dot(a, b, preferred_element_type=jnp.float32)
+
+    def push(l, steps, out, into, send_sems, recv_sems):
+        copies = []
+        for s in steps:
+            target = partner(me_dp, s, n_dp)
+            copies.append(
+                send(
+                    out.at[l, target],
+                    into.at[l, s],
+                    send_sems.at[l, s],
+                    recv_sems.at[l, s],
+                    "dp",
+                    target,
+                )
+            )
+        return copies
+
+    group = rows // state_rows
+    my_group = me_dp // group
+
+    def steps_of(g):
+        return [s for s in range(g * group, (g + 1) * group) if s]
+
+    def project(l, block, steps, where):
+        count = block.shape[0] // state_rows
+        sq_out[l, where] = lane_squares(block).reshape(count, state_rows, LANES)
+        copies = [push(l, steps, sq_out, sq_in, sq_send, sq_recv)]
+        scaled = (block * gains[l : l + 1]).astype(jnp.bfloat16)
         if l == 0:
             loads["win"].wait()
-        part = jnp.dot(scaled, win_v[l], preferred_element_type=jnp.float32)
-        val_out[l] = part.reshape(n_dp, state_rows, chans).astype(jnp.bfloat16)
-        val_copies = scatter(
-            val_out.at[l], val_in.at[l], val_send.at[l], val_recv.at[l], "dp", me_dp, n_dp
-        )
+        part = dot(scaled, win_v[l]).reshape(count, state_rows, chans)
+        val_out[l, where] = part.astype(jnp.bfloat16)
+        copies.append(push(l, steps, val_out, val_in, val_send, val_recv))
         if l == 0:
             loads["wgate"].wait()
-        part = jnp.dot(scaled, wgate_v[l], preferred_element_type=jnp.float32)
-        gate_out[l] = part.reshape(n_dp, state_rows, chans).astype(jnp.bfloat16)
-        gate_copies = scatter(
-            gate_out.at[l], gate_in_buf.at[l], gate_send.at[l], gate_recv.at[l], "dp", me_dp, n_dp
-        )
-
+        part = dot(scaled, wgate_v[l]).reshape(count, state_rows, chans)
+        gate_out[l, where] = part.astype(jnp.bfloat16)
+        copies.append(push(l, steps, gate_out, gate_in_buf, gate_send, gate_recv))
+        return copies
+
+    flying = project(0, current, order_of(n_dp), slice(None))
+    late = []
+
+    for l in range(layers):
+        sq_copies, val_copies, gate_copies = flying
         if l == 0:
             for name in ("cw", "cs", "rs", "wrec", "winj"):
                 loads[name].wait()
@@ -256,32 +278,81 @@
             gate = gate + gate_in_buf[l, s].astype(jnp.float32)
         gate = gate * scale
         read_all[l, me_dp] = (hidden * jax.nn.gelu(gate)).astype(jnp.bfloat16)
-        arrive(
-            gather(read_all.at[l], read_send.at[l], read_recv.at[l], "dp", me_dp, n_dp)
+        read_copies = dict(
+            zip(
+                order_of(n_dp),
+                gather(read_all.at[l], read_send.at[l], read_recv.at[l], "dp", me_dp, n_dp),
+            )
         )
-        reads = read_all[l].astype(jnp.float32).reshape(all_rows, chans).astype(jnp.bfloat16)
         if l == 0:
             loads["wout"].wait()
-        branch = jnp.dot(reads, wout_v[l], preferred_element_type=jnp.float32)
+        residual = x_all if l == 0 else x_keep.at[l - 1]
+        parts = []
+        for g in range(n_tp):
+            owner = partner(my_group, g, n_tp)
+            arrive([read_copies[s] for s in steps_of(g)])
+            reads = read_all[l, pl.ds(owner * group, group)].astype(jnp.float32)
+            reads = reads.reshape(rows, chans).astype(jnp.bfloat16)
+            branch = dot(reads, wout_v[l]).astype(jnp.bfloat16)
+            if l < layers - 1:
+                mine = part_all.at[l, me_tp, owner]
+                mine[...] = branch
+                copies = []
+                for s in order_of(n_tp):
+                    copies.append(
+                        send(
+                            mine,
+                            mine,
+                            part_send.at[l, g, s],
+                            part_recv.at[l, g, s],
+                            "tp",
+                            partner(me_tp, s, n_tp),
+                        )
+                    )
+                parts.append(copies)
+            else:
+                last_out[owner] = branch
+                copy = pltpu.make_async_remote_copy(
+                    src_ref=last_out.at[owner],
+                    dst_ref=last_in.at[me_tp],
+                    send_sem=last_send.at[g],
+                    recv_sem=last_recv.at[me_tp],
+                    device_id={"tp": owner},
+                    device_id_type=MESH,
+                )
+                late.append((owner, copy))
+                pl.when(owner != me_tp)(copy.start)
         if l < layers - 1:
-            part_all[l, me_tp] = branch.astype(jnp.bfloat16)
-            arrive(
-                gather(part_all.at[l], part_send.at[l], part_recv.at[l], "tp", me_tp, n_tp)
-            )
-            for j in range(n_tp):
-                current = current + part_all[l, j].astype(jnp.float32)
-            current = current.astype(jnp.bfloat16)
-            x_keep[...] = current.reshape(n_tp, rows, width)
-            current = current.astype(jnp.float32)
+            flying = [[], [], []]
+            for g in range(n_tp):
+                owner = partner(my_group, g, n_tp)
+                arrive(parts[g])
+                block = residual[owner].astype(jnp.float32)
+                for t in range(n_tp):
+                    block = block + part_all[l, t, owner].astype(jnp.float32)
+                block = block.astype(jnp.bfloat16)
+                x_keep[l, owner] = block
+                copies = project(
+                    l + 1, block.astype(jnp.float32), steps_of(g), pl.ds(owner * group, group)
+                )
+                for kind, more in zip(flying, copies):
+                    kind.extend(more)
         else:
-            last_out[...] = branch.reshape(n_tp, rows, width).astype(jnp.bfloat16)
-            arrive(
-                scatter(last_out, last_in, part_send.at[l], part_recv.at[l], "tp", me_tp, n_tp)
-            )
-            final = (x_keep if l else x_all)[me_tp].astype(jnp.float32) + last_out[me_tp].astype(jnp.float32)
+            final = residual[me_tp].astype(jnp.float32) + last_out[me_tp].astype(jnp.float32)
             for s in range(1, n_tp):
-                final = final + last_in[s].astype(jnp.float32)
+                other = partner(me_tp, s, n_tp)
+                pltpu.make_async_remote_copy(
+                    src_ref=last_out.at[other],
+                    dst_ref=last_in.at[other],
+                    send_sem=last_send.at[s],
+                    recv_sem=last_recv.at[other],
+                    device_id={"tp": other},
+                    device_id_type=MESH,
+                ).wait_recv()
+                final = final + last_in[other].astype(jnp.float32)
             mixed[...] = final.astype(jnp.bfloat16)
+    for owner, copy in late:
+        pl.when(owner != me_tp)(copy.wait_send)
     for copy in sent:
         copy.wait_send()
 
@@ -330,7 +401,7 @@
             like(conv_state),
             like(rec_state),
             pltpu.VMEM((n_tp, rows, width), bf16),
-            pltpu.VMEM((n_tp, rows, width), bf16),
+            pltpu.VMEM((layers, n_tp, rows, width), bf16),
             pltpu.VMEM((layers, n_dp, state_rows, LANES), f32),
             pltpu.VMEM((layers, n_dp, state_rows, LANES), f32),
             pltpu.VMEM((layers, n_dp, state_rows, chans), bf16),
@@ -338,7 +409,7 @@
             pltpu.VMEM((layers, n_dp, state_rows, chans), bf16),
             pltpu.VMEM((layers, n_dp, state_rows, chans), bf16),
             pltpu.VMEM((layers, n_dp, state_rows, chans), bf16),
-            pltpu.VMEM((layers, n_tp, all_rows, width), bf16),
+            pltpu.VMEM((layers, n_tp, n_tp, rows, width), bf16),
             pltpu.VMEM((n_tp, rows, width), bf16),
             pltpu.VMEM((n_tp, rows, width), bf16),
             dma((12,)),
@@ -352,8 +423,10 @@
             dma((layers, n_dp)),
             dma((layers, n_dp)),
             dma((layers, n_dp)),
-            dma((layers, n_tp)),
-            dma((layers, n_tp)),
+            dma((layers, n_tp, n_tp)),
+            dma((layers, n_tp, n_tp)),
+            dma((n_tp,)),
+            dma((n_tp,)),
         ],
         compiler_params=pltpu.CompilerParams(collective_id=0, has_side_effects=True),
     )(*args)

time: 37.4 us -> 34.7 us (0.928)
  Pallas kernels: 36.5 us -> 33.8 us
    pallas_call x1, Pallas kernels: 35.9 us -> 33.1 us  [body(): pl.pallas_call(functools.partial(kernel, n_tp, n_dp), out_shape=tuple((pl...]
where the time goes in v3:
time: 34.7 us; the launch traced here: 34.4 us
  Pallas kernels  33.8 us (97%)
  between operations  0.64 us (2%)
    pallas_call x1, Pallas kernels, body(): pl.pallas_call(functools.partial(kernel, n_tp, n_dp), out_shape=tuple((pl...  33.1 us

profile of v3, /device:TPU:0, one launch (start us, length us, event | category | flops | bytes accessed | tf_op | source)
XLA Modules:
  0.0 34.4 jit_solution(1041337851235311410)
XLA Ops:
  0.6 33.1 %shard_map.139 = (bf16[16,512]{1,0:T(8,128)(2,1)S(1)}, bf16[2,3,8,512]{3,2,1,0:T(8,128)(2,1)S(1)}, f32[2,8,512]{2,1,0:T(8,128)S(1)}) custom-call(bf16[16,512]{1,0:T(8,128)(2,1)} %tokens.1, f32[2,512]{1,0:T(2,128)} %norm_gain.1, bf16[2,512,512]{2,1,0:T(8,128)(2,1)} %w_input.1, bf16[2,512,512]{2,1,0:T(8,128)(2,1)} %w_gate.1, bf16[2,4,128,128]{3,2,1,0:T(8,128)(2,1)} %w_recur.1, ...), custom_call_target="tpu_custom_call" | custom-call | tf_op jit(solution)/shard_map/pallas_call | solution.py:386
  33.8 0.7 %shard_map.140 = (bf16[16,512]{1,0:T(8,128)(2,1)}, bf16[2,3,8,512]{3,2,1,0:T(8,128)(2,1)}, f32[2,8,512]{2,1,0:T(8,128)}) custom-call(bf16[16,512]{1,0:T(8,128)(2,1)S(1)} %get-tuple-element.6.refs_0_, bf16[2,3,8,512]{3,2,1,0:T(8,128)(2,1)S(1)} %get-tuple-element.7.refs_1_, f32[2,8,512]{2,1,0:T(8,128)S(1)} %get-tuple-element.8.refs_2_), custom_call_target="tpu_custom_call" | custom-call | tf_op jit(solution)/shard_map/pallas_call | solution.py:433
